TPU v7x, 32 devices: a whole 2x2x4 slice. The times are simulated.
32 devices in a mesh: fs: 16 (over z, y, x), tp: 2 (over core).
Axes of the slice: x: 2, y: 2, z: 4, core: 2. Of those that a mesh axis runs over, the one named last changes fastest.
Arguments:
- tokens: bfloat16 [6144, 2048], P('fs', 'tp'), may hold values from -8 to 8
- w_value: bfloat16 [2048, 1024], P('fs', 'tp'), may hold values from -0.125 to 0.125
- w_gate: bfloat16 [2048, 1024], P('fs', 'tp'), may hold values from -0.125 to 0.125
- conv_kernel: bfloat16 [31, 1024], replicated, may hold values from -1 to 1
- conv_gain: float32 [1024], replicated, may hold values from 0.1 to 1.9
- w_mix_out: bfloat16 [1024, 2048], P('fs', 'tp'), may hold values from -0.1875 to 0.1875
- mix_gain: float32 [2048], replicated, may hold values from 0.1 to 1.9
- w_up: bfloat16 [2048, 8192], P('fs', 'tp'), may hold values from -0.125 to 0.125
- w_down: bfloat16 [8192, 2048], P('tp', 'fs'), may hold values from -0.0625 to 0.0625
- out_gain: float32 [2048], replicated, may hold values from 0.1 to 1.9
Outputs:
- result: bfloat16 [6144, 2048], P('fs', 'tp')
All inputs are finite; a program needn't handle non-finite values.
Results may differ from a plain program's by a relative error of at most 0.013.
Values may be sent and summed in bfloat16 or wider, within the bound.
A program may use at most 128 MiB of HBM per device.

v0:
```python
import functools
import jax
import jax.numpy as jnp
from jax import lax
from jax.sharding import PartitionSpec as P


KERNEL = 31
LENGTH = 128


norm_eps = 1e-05
residual_scale = 2.0**0.5


def causal_filter(gated, kernel):
    sequences = gated.shape[0] // LENGTH
    frames = gated.astype(jnp.float32).reshape(sequences, LENGTH, gated.shape[1])
    padded = jnp.pad(frames, ((0, 0), (KERNEL - 1, 0), (0, 0)))
    accumulated = jnp.zeros(frames.shape, jnp.float32)
    for offset in range(KERNEL):
        accumulated = (
            accumulated + kernel[offset].astype(jnp.float32) * padded[:, offset : offset + LENGTH]
        )
    return accumulated.reshape(gated.shape[0], gated.shape[1])


def normalize(values, total_sum, total_sq, entries, gain_vector):
    average = total_sum / entries
    spread = jnp.maximum(total_sq / entries - average * average, 0.0)
    return (values - average[:, None]) * lax.rsqrt(spread[:, None] + norm_eps) * gain_vector


PLANE = 4


def layer(
    n_fs,
    n_tp,
    tokens,
    w_value,
    w_gate,
    conv_kernel,
    conv_gain,
    w_mix_out,
    mix_gain,
    w_up,
    w_down,
    out_gain,
):
    lines = n_fs // PLANE
    fs_rank = lax.axis_index("fs")
    line, place = fs_rank // PLANE, fs_rank % PLANE
    tp_rank = lax.axis_index("tp")
    frames, width_part = tokens.shape
    channel_part = w_value.shape[1]
    width, channels = width_part * n_tp, channel_part * n_tp

    def swap(array, mask):
        pairs = [(f, (f // PLANE) * PLANE + ((f % PLANE) ^ mask)) for f in range(n_fs)]
        return lax.ppermute(array, "fs", pairs)

    def shift(array, step, upward, first=0):
        if upward:
            moves = [(a, a + step) for a in range(first, lines - step)]
        else:
            moves = [(a, a - step) for a in range(step, lines - first)]
        pairs = [(a * PLANE + q, b * PLANE + q) for a, b in moves for q in range(PLANE)]
        return lax.ppermute(array, "fs", pairs)

    def put(buffer, block, index, axis=0):
        return lax.dynamic_update_slice_in_dim(buffer, jnp.expand_dims(block, axis), index, axis)

    def line_gather(block, direct):
        ups, downs = [block], [block]
        for step in range(1, lines):
            if step <= direct:
                ups.append(shift(block, step, True))
                downs.append(shift(block, step, False))
            else:
                ups.append(shift(ups[-1], 1, True, step - 1))
                downs.append(shift(downs[-1], 1, False, step - 1))
        out = put(jnp.zeros((lines,) + block.shape, block.dtype), block, line)
        for step in range(1, lines):
            piece = jnp.where(line >= step, ups[step], downs[lines - step])
            out = put(out, piece, (line - step) % lines)
        return out

    def plane_gather(block, axis):
        across, along = swap(block, 1), swap(block, 2)
        half = block.shape[0] // 2
        far = jnp.concatenate([swap(along[:half], 1), swap(across[half:], 2)], 0)
        shape = block.shape[:axis] + (PLANE,) + block.shape[axis:]
        out = jnp.zeros(shape, block.dtype)
        for mask, piece in enumerate((block, across, along, far)):
            out = put(out, piece, place ^ mask, axis)
        return out

    def tp_shift(block, step):
        return lax.ppermute(block, "tp", [(i, (i + step) % n_tp) for i in range(n_tp)])

    def tp_dot(block, weights):
        parts = weights.reshape((n_tp, -1) + weights.shape[1:])
        total = None
        for step in range(n_tp):
            piece = block if step == 0 else tp_shift(block, step)
            rows_at = lax.dynamic_index_in_dim(parts, (tp_rank - step) % n_tp, 0, False)
            term = jnp.dot(piece, rows_at, preferred_element_type=jnp.float32)
            total = term if total is None else total + term
        return total

    def plane_exchange(pieces):
        own = lax.dynamic_index_in_dim(pieces, place, 0, False)
        out = put(jnp.zeros_like(pieces), own, place)
        for mask in range(1, PLANE):
            sent = lax.dynamic_index_in_dim(pieces, place ^ mask, 0, False)
            came = swap(sent, mask)
            out = put(out, came, place ^ mask)
        return out

    pair_block = jnp.concatenate([w_value, w_gate], 1)
    pair_whole = plane_gather(line_gather(pair_block, lines), 1).reshape(width, 2 * channel_part)
    rows = w_value.shape[0]
    mix_whole = plane_gather(line_gather(w_mix_out, lines), 1).reshape(channels, width_part)

    units = w_up.shape[1]
    quarter = units // PLANE
    up_pieces = jnp.swapaxes(w_up.reshape(rows, PLANE, quarter), 0, 1)
    up_chunk = plane_exchange(up_pieces).reshape(PLANE * rows, quarter)
    up_whole = line_gather(up_chunk, 2).reshape(width, quarter)
    cols = w_down.shape[1]
    down_pieces = w_down.reshape(PLANE, quarter, cols)
    down_chunk = jnp.swapaxes(plane_exchange(down_pieces), 0, 1).reshape(quarter, PLANE * cols)
    down_whole = line_gather(down_chunk, 2)

    both = tp_dot(tokens, pair_whole)
    values_proj, gate_proj = both[:, :channel_part], both[:, channel_part:]
    gated = (values_proj * jax.nn.sigmoid(gate_proj)).astype(jnp.bfloat16)
    kernel = lax.dynamic_slice_in_dim(conv_kernel, tp_rank * channel_part, channel_part, 1)
    filtered = causal_filter(gated, kernel)
    channel_sum, channel_sq = lax.psum(
        (jnp.sum(filtered, 1), jnp.sum(filtered * filtered, 1)), "tp"
    )
    channel_gain = lax.dynamic_slice_in_dim(conv_gain, tp_rank * channel_part, channel_part, 0)
    activated = jax.nn.silu(
        normalize(filtered, channel_sum, channel_sq, channels, channel_gain)
    ).astype(jnp.bfloat16)
    mixed = tp_dot(activated, mix_whole)
    combined = residual_scale * tokens.astype(jnp.float32) + mixed
    middle_sum, middle_sq = lax.psum((jnp.sum(combined, 1), jnp.sum(combined * combined, 1)), "tp")
    middle_gain = lax.dynamic_slice_in_dim(mix_gain, tp_rank * width_part, width_part, 0)
    middle = normalize(combined, middle_sum, middle_sq, width, middle_gain).astype(jnp.bfloat16)

    plane_part = plane_gather(middle, 0).reshape(PLANE * frames, width_part)
    hidden = jnp.square(jax.nn.relu(tp_dot(plane_part, up_whole))).astype(jnp.bfloat16)

    per_core = lines // n_tp

    def product(core, at):
        weights = lax.dynamic_index_in_dim(down_whole, core * per_core + at, 0, False)
        return jnp.dot(hidden, weights, preferred_element_type=jnp.float32)

    came = []
    for step in range(1, n_tp):
        sent = [product((tp_rank + step) % n_tp, at) for at in range(per_core)]
        came.append([tp_shift(piece.astype(jnp.bfloat16), step) for piece in sent])
    chunks = []
    for at in range(per_core):
        chunk = product(tp_rank, at)
        for arrived in came:
            chunk = chunk + arrived[at].astype(jnp.float32)
        chunks.append(chunk.reshape(PLANE, frames, PLANE * cols))

    def of_place(part, mask):
        return lax.dynamic_index_in_dim(part, place ^ mask, 0, False)

    def plane_sum(part, mask_first, mask_second):
        sent = jnp.stack([of_place(part, mask_first), of_place(part, 3)]).astype(jnp.bfloat16)
        arrived = swap(sent, mask_first).astype(jnp.float32)
        onward = (of_place(part, mask_second) + arrived[1]).astype(jnp.bfloat16)
        return of_place(part, 0) + arrived[0] + swap(onward, mask_second).astype(jnp.float32)

    down_sum = jnp.concatenate(
        [
            plane_sum(chunk, 1, 2) if at % 2 == 0 else plane_sum(chunk, 2, 1)
            for at, chunk in enumerate(chunks)
        ],
        1,
    )
    final = residual_scale * middle.astype(jnp.float32) + down_sum
    final_sum, final_sq = lax.psum((jnp.sum(final, 1), jnp.sum(final * final, 1)), "tp")
    final_gain = lax.dynamic_slice_in_dim(out_gain, tp_rank * width_part, width_part, 0)
    return normalize(final, final_sum, final_sq, width, final_gain).astype(jnp.bfloat16)


def solution(mesh):
    in_specs = (
        P("fs", "tp"),
        P("fs", "tp"),
        P("fs", "tp"),
        P(),
        P(),
        P("fs", "tp"),
        P(),
        P("fs", "tp"),
        P("tp", "fs"),
        P(),
    )
    out_specs = P("fs", "tp")
    return jax.shard_map(
        functools.partial(layer, mesh.shape["fs"], mesh.shape["tp"]),
        mesh=mesh,
        in_specs=in_specs,
        out_specs=out_specs,
        check_vma=False,
    )
```

profile of v0, /device:TPU:0, one launch (start us, length us, event | category | flops | bytes accessed | tf_op | source)
XLA Modules:
  0.0 423.5 jit_solution(14258402920119980455)
XLA Ops:
  1.9 5.0 %collective-permute-start = (bf16[128,1024]{1,0:T(8,128)(2,1)S(1)}, bf16[128,1024]{1,0:T(8,128)(2,1)S(1)}, u32[]{:S(2)}, u32[]{:S(2)}) collective-permute-start(bf16[128,1024]{1,0:T(8,128)(2,1)S(1)} %constant_dynamic-update-slice_fusion.4), channel_id=1, source_target_pairs={{0,8},{2,10},{4,12},{6,14},{8,16},{10,18},{12,20},{14,22},{16,24},... | collective-permute-start | bytes 786440 | tf_op jit(solution)/shard_map/ppermute | solution.py:69
  8.2 3.9 collective-permute-start.2
  12.1 5.0 %collective-permute-start.11 = (bf16[64,1024]{1,0:T(8,128)(2,1)}, bf16[64,1024]{1,0:T(8,128)(2,1)S(1)}, u32[]{:S(2)}, u32[]{:S(2)}) collective-permute-start(bf16[64,1024]{1,0:T(8,128)(2,1)} %param.15), channel_id=1, source_target_pairs={{0,8},{2,10},{4,12},{6,14},{8,16},{10,18},{12,20},{14,22},{16,24},... | collective-permute-start | bytes 393224 | tf_op jit(solution)/shard_map/ppermute | solution.py:69
  26.0 5.9 %collective-permute-start.13 = (bf16[64,1024]{1,0:T(8,128)(2,1)S(1)}, bf16[64,1024]{1,0:T(8,128)(2,1)S(1)}, u32[]{:S(2)}, u32[]{:S(2)}) collective-permute-start(bf16[64,1024]{1,0:T(8,128)(2,1)S(1)} %copy-done.7), channel_id=1, source_target_pairs={{0,16},{2,18},{4,20},{6,22},{8,24},{10,26},{12,28},{14,30},{1,17},... | collective-permute-start | bytes 393224 | tf_op jit(solution)/shard_map/ppermute | solution.py:69
  34.8 7.5 %collective-permute-start.15 = (bf16[64,1024]{1,0:T(8,128)(2,1)S(1)}, bf16[64,1024]{1,0:T(8,128)(2,1)S(1)}, u32[]{:S(2)}, u32[]{:S(2)}) collective-permute-start(bf16[64,1024]{1,0:T(8,128)(2,1)S(1)} %copy-done.7), channel_id=1, source_target_pairs={{0,24},{2,26},{4,28},{6,30},{1,25},{3,27},{5,29},{7,31}} | collective-permute-start | bytes 393224 | tf_op jit(solution)/shard_map/ppermute | solution.py:69
  46.1 4.9 %collective-permute-done.16 = bf16[64,1024]{1,0:T(8,128)(2,1)S(1)} collective-permute-done((bf16[64,1024]{1,0:T(8,128)(2,1)S(1)}, bf16[64,1024]{1,0:T(8,128)(2,1)S(1)}, u32[]{:S(2)}, u32[]{:S(2)}) %collective-permute-start.16) | collective-permute-done | bytes 131104 | tf_op jit(solution)/shard_map/ppermute | solution.py:69
  56.9 4.4 %collective-permute-done.3 = bf16[128,1024]{1,0:T(8,128)(2,1)S(1)} collective-permute-done((bf16[128,1024]{1,0:T(8,128)(2,1)S(1)}, bf16[128,1024]{1,0:T(8,128)(2,1)S(1)}, u32[]{:S(2)}, u32[]{:S(2)}) %collective-permute-start.3) | collective-permute-done | bytes 262176 | tf_op jit(solution)/shard_map/ppermute | solution.py:69
  72.0 4.3 %collective-permute-done.18 = bf16[4,64,1024]{2,1,0:T(8,128)(2,1)S(1)} collective-permute-done((bf16[4,64,1024]{2,1,0:T(8,128)(2,1)}, bf16[4,64,1024]{2,1,0:T(8,128)(2,1)S(1)}, u32[]{:S(2)}, u32[]{:S(2)}) %collective-permute-start.18) | collective-permute-done | bytes 524320 | tf_op jit(solution)/shard_map/ppermute | solution.py:61
  78.0 21.5 %collective-permute-done.20 = bf16[2,64,1024]{2,1,0:T(8,128)(2,1)S(1)} collective-permute-done((bf16[2,64,1024]{2,1,0:T(8,128)(2,1)S(1)}, bf16[2,64,1024]{2,1,0:T(8,128)(2,1)S(1)}, u32[]{:S(2)}, u32[]{:S(2)}) %collective-permute-start.20) | collective-permute-done | bytes 262176 | tf_op jit(solution)/shard_map/ppermute | solution.py:61
  103.0 8.7 %collective-permute-done.9 = bf16[2,128,1024]{2,1,0:T(8,128)(2,1)S(1)} collective-permute-done((bf16[2,128,1024]{2,1,0:T(8,128)(2,1)S(1)}, bf16[2,128,1024]{2,1,0:T(8,128)(2,1)S(1)}, u32[]{:S(2)}, u32[]{:S(2)}) %collective-permute-start.9) | collective-permute-done | bytes 524320 | tf_op jit(solution)/shard_map/ppermute | solution.py:61
  116.8 3.5 fusion.124
  142.2 15.5 %collective-permute-done.26 = bf16[128,1024]{1,0:T(8,128)(2,1)} collective-permute-done((bf16[128,1024]{1,0:T(8,128)(2,1)}, bf16[128,1024]{1,0:T(8,128)(2,1)}, u32[]{:S(2)}, u32[]{:S(2)}) %collective-permute-start.26) | collective-permute-done | bytes 262176 | tf_op jit(solution)/shard_map/ppermute | solution.py:61
  169.0 6.5 %collective-permute-start.29 = (bf16[512,1024]{1,0:T(8,128)(2,1)S(1)}, bf16[512,1024]{1,0:T(8,128)(2,1)}, u32[]{:S(2)}, u32[]{:S(2)}) collective-permute-start(bf16[512,1024]{1,0:T(8,128)(2,1)S(1)} %bitcast.223), channel_id=1, source_target_pairs={{0,8},{2,10},{4,12},{6,14},{8,16},{10,18},{12,20},{14,22},{16,24},... | collective-permute-start | bytes 3145736 | tf_op jit(solution)/shard_map/ppermute | solution.py:69
  179.0 7.5 %collective-permute-start.32 = (bf16[512,1024]{1,0:T(8,128)(2,1)S(1)}, bf16[512,1024]{1,0:T(8,128)(2,1)}, u32[]{:S(2)}, u32[]{:S(2)}) collective-permute-start(bf16[512,1024]{1,0:T(8,128)(2,1)S(1)} %bitcast.225), channel_id=1, source_target_pairs={{0,16},{2,18},{4,20},{6,22},{8,24},{10,26},{12,28},{14,30},{1,17},... | collective-permute-start | bytes 3145736 | tf_op jit(solution)/shard_map/ppermute | solution.py:69
  193.0 6.0 %collective-permute-done.25 = bf16[192,1024]{1,0:T(8,128)(2,1)} collective-permute-done((bf16[192,1024]{1,0:T(8,128)(2,1)}, bf16[192,1024]{1,0:T(8,128)(2,1)}, u32[]{:S(2)}, u32[]{:S(2)}) %collective-permute-start.25) | collective-permute-done | bytes 393248 | tf_op jit(solution)/shard_map/ppermute | solution.py:61
  204.6 5.4 %collective-permute-done.24 = bf16[192,1024]{1,0:T(8,128)(2,1)S(1)} collective-permute-done((bf16[192,1024]{1,0:T(8,128)(2,1)S(1)}, bf16[192,1024]{1,0:T(8,128)(2,1)S(1)}, u32[]{:S(2)}, u32[]{:S(2)}) %collective-permute-start.24) | collective-permute-done | bytes 393248 | tf_op jit(solution)/shard_map/ppermute | solution.py:61
  212.0 11.4 %collective-permute-start.39 = (bf16[1024,512]{0,1:T(8,128)(2,1)S(1)}, bf16[1024,512]{0,1:T(8,128)(2,1)}, u32[]{:S(2)}, u32[]{:S(2)}) collective-permute-start(bf16[1024,512]{0,1:T(8,128)(2,1)S(1)} %bitcast.229), channel_id=1, source_target_pairs={{0,8},{2,10},{4,12},{6,14},{8,16},{10,18},{12,20},{14,22},{16,24},... | collective-permute-start | bytes 3145736 | tf_op jit(solution)/shard_map/ppermute | solution.py:69
  223.4 23.1 %collective-permute-done.30 = bf16[512,1024]{1,0:T(8,128)(2,1)} collective-permute-done((bf16[512,1024]{1,0:T(8,128)(2,1)S(1)}, bf16[512,1024]{1,0:T(8,128)(2,1)}, u32[]{:S(2)}, u32[]{:S(2)}) %collective-permute-start.30) | collective-permute-done | bytes 1048608 | tf_op jit(solution)/shard_map/ppermute | solution.py:69
  250.5 18.5 %collective-permute-done.40 = bf16[1024,512]{0,1:T(8,128)(2,1)} collective-permute-done((bf16[1024,512]{0,1:T(8,128)(2,1)S(1)}, bf16[1024,512]{0,1:T(8,128)(2,1)}, u32[]{:S(2)}, u32[]{:S(2)}) %collective-permute-start.40) | collective-permute-done | bytes 1048608 | tf_op jit(solution)/shard_map/ppermute | solution.py:69
  272.9 18.6 %collective-permute-done.31 = bf16[512,1024]{1,0:T(8,128)(2,1)} collective-permute-done((bf16[512,1024]{1,0:T(8,128)(2,1)}, bf16[512,1024]{1,0:T(8,128)(2,1)}, u32[]{:S(2)}, u32[]{:S(2)}) %collective-permute-start.31) | collective-permute-done | bytes 1048608 | tf_op jit(solution)/shard_map/ppermute | solution.py:69
  295.2 18.8 %collective-permute-done.41 = bf16[1024,512]{0,1:T(8,128)(2,1)} collective-permute-done((bf16[1024,512]{0,1:T(8,128)(2,1)}, bf16[1024,512]{0,1:T(8,128)(2,1)}, u32[]{:S(2)}, u32[]{:S(2)}) %collective-permute-start.41) | collective-permute-done | bytes 1048608 | tf_op jit(solution)/shard_map/ppermute | solution.py:69
  319.6 16.7 %collective-permute-done.34 = bf16[512,1024]{1,0:T(8,128)(2,1)S(1)} collective-permute-done((bf16[512,1024]{1,0:T(8,128)(2,1)S(1)}, bf16[512,1024]{1,0:T(8,128)(2,1)S(1)}, u32[]{:S(2)}, u32[]{:S(2)}) %collective-permute-start.34) | collective-permute-done | bytes 1048608 | tf_op jit(solution)/shard_map/ppermute | solution.py:69
  336.8 21.9 %collective-permute-done.44 = bf16[1024,512]{0,1:T(8,128)(2,1)S(1)} collective-permute-done((bf16[1024,512]{0,1:T(8,128)(2,1)S(1)}, bf16[1024,512]{0,1:T(8,128)(2,1)S(1)}, u32[]{:S(2)}, u32[]{:S(2)}) %collective-permute-start.44) | collective-permute-done | bytes 1048608 | tf_op jit(solution)/shard_map/ppermute | solution.py:69
  359.2 6.9 %fusion = f32[1536,1024]{1,0:T(8,128)S(1)} fusion(bf16[1536,1024]{1,0:T(8,128)(2,1)} %collective-permute-done.35, bf16[2,1024,1024]{2,1,0:T(8,128)(2,1)S(1)} %bitcast.233, s32[]{:T(128)S(6)} %select_n.270), kind=kOutput, calls=%fused_computation.35 | convolution fusion | flops 3221225472 | bytes 11534340 | tf_op jit(solution)/shard_map/dot_general | solution.py:108
  366.1 4.3 %multiply_convert_fusion = bf16[1536,1024]{1,0:T(8,128)(2,1)S(1)} fusion(f32[1536,1024]{1,0:T(8,128)S(1)} %fusion, bf16[1536,1024]{1,0:T(8,128)(2,1)S(1)} %bitcast.236, bf16[2,1024,1024]{2,1,0:T(8,128)(2,1)S(1)} %bitcast.234, s32[]{:T(128)S(6)} %select_n.268), kind=kOutput, calls=%fused_computation | convolution fusion | flops 3227516928 | bytes 14680068 | tf_op jit(solution)/shard_map/dot_general | solution.py:108
  370.4 3.1 convolution_convert_fusion
  373.6 5.2 %convolution_convert_fusion.1 = bf16[1536,512]{1,0:T(8,128)(2,1)} fusion(bf16[1536,1024]{1,0:T(8,128)(2,1)} %copy-done.18, bf16[4,1024,512]{1,2,0:T(8,128)(2,1)} %copy-done.2, s32[]{:T(128)S(6)} %select_n.292), kind=kOutput, calls=%fused_computation.4 | convolution fusion | flops 1611399168 | bytes 5767172 | tf_op jit(solution)/shard_map/dot_general | solution.py:161
  379.3 4.6 %convert_add_fusion = f32[1536,512]{1,0:T(8,128)S(1)} fusion(bf16[1536,512]{1,0:T(8,128)(2,1)} %collective-permute-done.48, bf16[1536,1024]{1,0:T(8,128)(2,1)} %copy-done.18, bf16[4,1024,512]{1,2,0:T(8,128)(2,1)} %copy-done.2, s32[]{:T(128)S(6)} %select_n.293), kind=kOutput, calls=%fused_computation.1 | convolution fusion | flops 1612185600 | bytes 8912900 | tf_op jit(solution)/shard_map/dot_general | solution.py:161
  385.7 3.1 convert_add_fusion.1
  389.7 13.9 %collective-permute-done.49 = bf16[2,384,512]{2,1,0:T(8,128)(2,1)S(1)} collective-permute-done((bf16[2,384,512]{2,1,0:T(8,128)(2,1)S(1)}, bf16[2,384,512]{2,1,0:T(8,128)(2,1)S(1)}, u32[]{:S(2)}, u32[]{:S(2)}) %collective-permute-start.49) | collective-permute-done | bytes 786464 | tf_op jit(solution)/shard_map/ppermute | solution.py:61
  404.5 5.0 %collective-permute-done.46 = bf16[2,384,512]{2,1,0:T(8,128)(2,1)S(1)} collective-permute-done((bf16[2,384,512]{2,1,0:T(8,128)(2,1)S(1)}, bf16[2,384,512]{2,1,0:T(8,128)(2,1)S(1)}, u32[]{:S(2)}, u32[]{:S(2)}) %collective-permute-start.46) | collective-permute-done | bytes 786464 | tf_op jit(solution)/shard_map/ppermute | solution.py:61
  410.4 6.6 %collective-permute-done.50 = bf16[384,512]{1,0:T(8,128)(2,1)S(1)} collective-permute-done((bf16[384,512]{1,0:T(8,128)(2,1)S(1)}, bf16[384,512]{1,0:T(8,128)(2,1)S(1)}, u32[]{:S(2)}, u32[]{:S(2)}) %collective-permute-start.50) | collective-permute-done | bytes 393248 | tf_op jit(solution)/shard_map/ppermute | solution.py:61
  (214 shorter events, 125.1 us)
Async XLA Ops:
  1.9 52.0 %collective-permute-start = (bf16[128,1024]{1,0:T(8,128)(2,1)S(1)}, bf16[128,1024]{1,0:T(8,128)(2,1)S(1)}, u32[]{:S(2)}, u32[]{:S(2)}) collective-permute-start(bf16[128,1024]{1,0:T(8,128)(2,1)S(1)} %constant_dynamic-update-slice_fusion.4), channel_id=1, source_target_pairs={{0,8},{2,10},{4,12},{6,14},{8,16},{10,18},{12,20},{14,22},{16,24},... | collective-permute-start | bytes 786440 | tf_op jit(solution)/shard_map/ppermute | solution.py:69
  6.9 48.3 %collective-permute-start.1 = (bf16[128,1024]{1,0:T(8,128)(2,1)S(1)}, bf16[128,1024]{1,0:T(8,128)(2,1)S(1)}, u32[]{:S(2)}, u32[]{:S(2)}) collective-permute-start(bf16[128,1024]{1,0:T(8,128)(2,1)S(1)} %constant_dynamic-update-slice_fusion.4), channel_id=1, source_target_pairs={{24,0},{26,2},{28,4},{30,6},{25,1},{27,3},{29,5},{31,7}} | collective-permute-start | bytes 786440 | tf_op jit(solution)/shard_map/ppermute | solution.py:69
  8.2 47.1 %collective-permute-start.2 = (bf16[128,1024]{1,0:T(8,128)(2,1)S(1)}, bf16[128,1024]{1,0:T(8,128)(2,1)S(1)}, u32[]{:S(2)}, u32[]{:S(2)}) collective-permute-start(bf16[128,1024]{1,0:T(8,128)(2,1)S(1)} %constant_dynamic-update-slice_fusion.4), channel_id=1, source_target_pairs={{0,16},{2,18},{4,20},{6,22},{8,24},{10,26},{12,28},{14,30},{1,17},... | collective-permute-start | bytes 786440 | tf_op jit(solution)/shard_map/ppermute | solution.py:69
  55.2 57.9 %collective-permute-start.10 = (bf16[384,1024]{1,0:T(8,128)(2,1)}, bf16[384,1024]{1,0:T(8,128)(2,1)S(1)}, u32[]{:S(2)}, u32[]{:S(2)}) collective-permute-start(bf16[384,1024]{1,0:T(8,128)(2,1)} %param.10), channel_id=1, source_target_pairs={{0,1},{1,0},{2,3},{3,2},{4,5},{5,4},{6,7},{7,6},{8,9},{9,8},{10,11... | collective-permute-start | bytes 2359304 | tf_op jit(solution)/shard_map/ppermute | solution.py:100
  64.1 35.4 %collective-permute-start.6 = (bf16[4,128,1024]{2,1,0:T(8,128)(2,1)S(1)}, bf16[4,128,1024]{2,1,0:T(8,128)(2,1)S(1)}, u32[]{:S(2)}, u32[]{:S(2)}) collective-permute-start(bf16[4,128,1024]{2,1,0:T(8,128)(2,1)S(1)} %bitcast_dynamic-update-slice_fusion.21), channel_id=1, source_target_pairs={{0,2},{2,0},{4,6},{6,4},{8,10},{10,8},{12,14},{14,12},{16,18},{18,... | collective-permute-start | bytes 3145736 | tf_op jit(solution)/shard_map/ppermute | solution.py:61
  65.7 35.5 %collective-permute-start.7 = (bf16[4,128,1024]{2,1,0:T(8,128)(2,1)S(1)}, bf16[4,128,1024]{2,1,0:T(8,128)(2,1)S(1)}, u32[]{:S(2)}, u32[]{:S(2)}) collective-permute-start(bf16[4,128,1024]{2,1,0:T(8,128)(2,1)S(1)} %bitcast_dynamic-update-slice_fusion.21), channel_id=1, source_target_pairs={{0,4},{2,6},{4,0},{6,2},{8,12},{10,14},{12,8},{14,10},{16,20},{18,... | collective-permute-start | bytes 3145736 | tf_op jit(solution)/shard_map/ppermute | solution.py:61
  70.5 29.0 %collective-permute-start.20 = (bf16[2,64,1024]{2,1,0:T(8,128)(2,1)S(1)}, bf16[2,64,1024]{2,1,0:T(8,128)(2,1)S(1)}, u32[]{:S(2)}, u32[]{:S(2)}) collective-permute-start(bf16[2,64,1024]{2,1,0:T(8,128)(2,1)S(1)} %slice.298), channel_id=1, source_target_pairs={{0,4},{2,6},{4,0},{6,2},{8,12},{10,14},{12,8},{14,10},{16,20},{18,... | collective-permute-start | bytes 786440 | tf_op jit(solution)/shard_map/ppermute | solution.py:61
  76.3 23.1 %collective-permute-start.19 = (bf16[2,64,1024]{2,1,0:T(8,128)(2,1)S(1)}, bf16[2,64,1024]{2,1,0:T(8,128)(2,1)S(1)}, u32[]{:S(2)}, u32[]{:S(2)}) collective-permute-start(bf16[2,64,1024]{2,1,0:T(8,128)(2,1)S(1)} %slice.297), channel_id=1, source_target_pairs={{0,2},{2,0},{4,6},{6,4},{8,10},{10,8},{12,14},{14,12},{16,18},{18,... | collective-permute-start | bytes 786440 | tf_op jit(solution)/shard_map/ppermute | solution.py:61
  131.5 30.2 %collective-permute-start.22 = (bf16[384,1024]{1,0:T(8,128)(2,1)S(1)}, bf16[384,1024]{1,0:T(8,128)(2,1)}, u32[]{:S(2)}, u32[]{:S(2)}) collective-permute-start(bf16[384,1024]{1,0:T(8,128)(2,1)S(1)} %get-tuple-element.18), channel_id=1, source_target_pairs={{0,2},{2,0},{4,6},{6,4},{8,10},{10,8},{12,14},{14,12},{16,18},{18,... | collective-permute-start | bytes 2359304 | tf_op jit(solution)/shard_map/ppermute | solution.py:61
  134.0 23.7 %collective-permute-start.26 = (bf16[128,1024]{1,0:T(8,128)(2,1)}, bf16[128,1024]{1,0:T(8,128)(2,1)}, u32[]{:S(2)}, u32[]{:S(2)}) collective-permute-start(bf16[128,1024]{1,0:T(8,128)(2,1)} %bitcast.75), channel_id=1, source_target_pairs={{0,2},{2,0},{4,6},{6,4},{8,10},{10,8},{12,14},{14,12},{16,18},{18,... | collective-permute-start | bytes 786440 | tf_op jit(solution)/shard_map/ppermute | solution.py:61
  136.3 22.8 %collective-permute-start.27 = (bf16[128,1024]{1,0:T(8,128)(2,1)}, bf16[128,1024]{1,0:T(8,128)(2,1)}, u32[]{:S(2)}, u32[]{:S(2)}) collective-permute-start(bf16[128,1024]{1,0:T(8,128)(2,1)} %bitcast.77), channel_id=1, source_target_pairs={{0,4},{2,6},{4,0},{6,2},{8,12},{10,14},{12,8},{14,10},{16,20},{18,... | collective-permute-start | bytes 786440 | tf_op jit(solution)/shard_map/ppermute | solution.py:61
  137.7 27.2 %collective-permute-start.28 = (bf16[128,1024]{1,0:T(8,128)(2,1)}, bf16[128,1024]{1,0:T(8,128)(2,1)}, u32[]{:S(2)}, u32[]{:S(2)}) collective-permute-start(bf16[128,1024]{1,0:T(8,128)(2,1)} %bitcast.79), channel_id=1, source_target_pairs={{0,6},{2,4},{4,2},{6,0},{8,14},{10,12},{12,10},{14,8},{16,22},{18,... | collective-permute-start | bytes 786440 | tf_op jit(solution)/shard_map/ppermute | solution.py:61
  140.0 28.9 %collective-permute-start.36 = (bf16[1024,128]{1,0:T(8,128)(2,1)}, bf16[1024,128]{1,0:T(8,128)(2,1)}, u32[]{:S(2)}, u32[]{:S(2)}) collective-permute-start(bf16[1024,128]{1,0:T(8,128)(2,1)} %get-tuple-element.26), channel_id=1, source_target_pairs={{0,2},{2,0},{4,6},{6,4},{8,10},{10,8},{12,14},{14,12},{16,18},{18,... | collective-permute-start | bytes 786440 | tf_op jit(solution)/shard_map/ppermute | solution.py:61
  157.7 18.9 %collective-permute-start.37 = (bf16[1024,128]{1,0:T(8,128)(2,1)S(1)}, bf16[1024,128]{1,0:T(8,128)(2,1)}, u32[]{:S(2)}, u32[]{:S(2)}) collective-permute-start(bf16[1024,128]{1,0:T(8,128)(2,1)S(1)} %get-tuple-element.25), channel_id=1, source_target_pairs={{0,4},{2,6},{4,0},{6,2},{8,12},{10,14},{12,8},{14,10},{16,20},{18,... | collective-permute-start | bytes 786440 | tf_op jit(solution)/shard_map/ppermute | solution.py:61
  159.2 19.8 %collective-permute-start.38 = (bf16[1024,128]{1,0:T(8,128)(2,1)}, bf16[1024,128]{1,0:T(8,128)(2,1)}, u32[]{:S(2)}, u32[]{:S(2)}) collective-permute-start(bf16[1024,128]{1,0:T(8,128)(2,1)} %get-tuple-element.24), channel_id=1, source_target_pairs={{0,6},{2,4},{4,2},{6,0},{8,14},{10,12},{12,10},{14,8},{16,22},{18,... | collective-permute-start | bytes 786440 | tf_op jit(solution)/shard_map/ppermute | solution.py:61
  161.7 28.9 %collective-permute-start.23 = (bf16[384,1024]{1,0:T(8,128)(2,1)S(1)}, bf16[384,1024]{1,0:T(8,128)(2,1)}, u32[]{:S(2)}, u32[]{:S(2)}) collective-permute-start(bf16[384,1024]{1,0:T(8,128)(2,1)S(1)} %get-tuple-element.18), channel_id=1, source_target_pairs={{0,4},{2,6},{4,0},{6,2},{8,12},{10,14},{12,8},{14,10},{16,20},{18,... | collective-permute-start | bytes 2359304 | tf_op jit(solution)/shard_map/ppermute | solution.py:61
  164.9 34.0 %collective-permute-start.25 = (bf16[192,1024]{1,0:T(8,128)(2,1)}, bf16[192,1024]{1,0:T(8,128)(2,1)}, u32[]{:S(2)}, u32[]{:S(2)}) collective-permute-start(bf16[192,1024]{1,0:T(8,128)(2,1)} %slice.300), channel_id=1, source_target_pairs={{0,4},{2,6},{4,0},{6,2},{8,12},{10,14},{12,8},{14,10},{16,20},{18,... | collective-permute-start | bytes 1179656 | tf_op jit(solution)/shard_map/ppermute | solution.py:61
  169.0 43.0 %collective-permute-start.29 = (bf16[512,1024]{1,0:T(8,128)(2,1)S(1)}, bf16[512,1024]{1,0:T(8,128)(2,1)}, u32[]{:S(2)}, u32[]{:S(2)}) collective-permute-start(bf16[512,1024]{1,0:T(8,128)(2,1)S(1)} %bitcast.223), channel_id=1, source_target_pairs={{0,8},{2,10},{4,12},{6,14},{8,16},{10,18},{12,20},{14,22},{16,24},... | collective-permute-start | bytes 3145736 | tf_op jit(solution)/shard_map/ppermute | solution.py:69
  176.6 70.0 %collective-permute-start.30 = (bf16[512,1024]{1,0:T(8,128)(2,1)S(1)}, bf16[512,1024]{1,0:T(8,128)(2,1)}, u32[]{:S(2)}, u32[]{:S(2)}) collective-permute-start(bf16[512,1024]{1,0:T(8,128)(2,1)S(1)} %bitcast.224), channel_id=1, source_target_pairs={{16,0},{18,2},{20,4},{22,6},{24,8},{26,10},{28,12},{30,14},{17,1},... | collective-permute-start | bytes 3145736 | tf_op jit(solution)/shard_map/ppermute | solution.py:69
  179.0 68.9 %collective-permute-start.32 = (bf16[512,1024]{1,0:T(8,128)(2,1)S(1)}, bf16[512,1024]{1,0:T(8,128)(2,1)}, u32[]{:S(2)}, u32[]{:S(2)}) collective-permute-start(bf16[512,1024]{1,0:T(8,128)(2,1)S(1)} %bitcast.225), channel_id=1, source_target_pairs={{0,16},{2,18},{4,20},{6,22},{8,24},{10,26},{12,28},{14,30},{1,17},... | collective-permute-start | bytes 3145736 | tf_op jit(solution)/shard_map/ppermute | solution.py:69
  190.6 78.4 %collective-permute-start.40 = (bf16[1024,512]{0,1:T(8,128)(2,1)S(1)}, bf16[1024,512]{0,1:T(8,128)(2,1)}, u32[]{:S(2)}, u32[]{:S(2)}) collective-permute-start(bf16[1024,512]{0,1:T(8,128)(2,1)S(1)} %bitcast.228), channel_id=1, source_target_pairs={{16,0},{18,2},{20,4},{22,6},{24,8},{26,10},{28,12},{30,14},{17,1},... | collective-permute-start | bytes 3145736 | tf_op jit(solution)/shard_map/ppermute | solution.py:69
  212.0 147.2 %collective-permute-start.35 = (bf16[1536,1024]{1,0:T(8,128)(2,1)}, bf16[1536,1024]{1,0:T(8,128)(2,1)}, u32[]{:S(2)}, u32[]{:S(2)}) collective-permute-start(bf16[1536,1024]{1,0:T(8,128)(2,1)} %bitcast.235), channel_id=1, source_target_pairs={{0,1},{1,0},{2,3},{3,2},{4,5},{5,4},{6,7},{7,6},{8,9},{9,8},{10,11... | collective-permute-start | bytes 9437192 | tf_op jit(solution)/shard_map/ppermute | solution.py:100
  212.0 59.6 %collective-permute-start.39 = (bf16[1024,512]{0,1:T(8,128)(2,1)S(1)}, bf16[1024,512]{0,1:T(8,128)(2,1)}, u32[]{:S(2)}, u32[]{:S(2)}) collective-permute-start(bf16[1024,512]{0,1:T(8,128)(2,1)S(1)} %bitcast.229), channel_id=1, source_target_pairs={{0,8},{2,10},{4,12},{6,14},{8,16},{10,18},{12,20},{14,22},{16,24},... | collective-permute-start | bytes 3145736 | tf_op jit(solution)/shard_map/ppermute | solution.py:69
  246.5 44.9 %collective-permute-start.31 = (bf16[512,1024]{1,0:T(8,128)(2,1)}, bf16[512,1024]{1,0:T(8,128)(2,1)}, u32[]{:S(2)}, u32[]{:S(2)}) collective-permute-start(bf16[512,1024]{1,0:T(8,128)(2,1)} %collective-permute-done.30), channel_id=1, source_target_pairs={{8,0},{10,2},{12,4},{14,6},{9,1},{11,3},{13,5},{15,7}} | collective-permute-start | bytes 3145736 | tf_op jit(solution)/shard_map/ppermute | solution.py:69
  247.8 46.0 %collective-permute-start.42 = (bf16[1024,512]{0,1:T(8,128)(2,1)S(1)}, bf16[1024,512]{0,1:T(8,128)(2,1)}, u32[]{:S(2)}, u32[]{:S(2)}) collective-permute-start(bf16[1024,512]{0,1:T(8,128)(2,1)S(1)} %bitcast.230), channel_id=1, source_target_pairs={{0,16},{2,18},{4,20},{6,22},{8,24},{10,26},{12,28},{14,30},{1,17},... | collective-permute-start | bytes 3145736 | tf_op jit(solution)/shard_map/ppermute | solution.py:69
  269.0 44.9 %collective-permute-start.41 = (bf16[1024,512]{0,1:T(8,128)(2,1)}, bf16[1024,512]{0,1:T(8,128)(2,1)}, u32[]{:S(2)}, u32[]{:S(2)}) collective-permute-start(bf16[1024,512]{0,1:T(8,128)(2,1)} %collective-permute-done.40), channel_id=1, source_target_pairs={{8,0},{10,2},{12,4},{14,6},{9,1},{11,3},{13,5},{15,7}} | collective-permute-start | bytes 3145736 | tf_op jit(solution)/shard_map/ppermute | solution.py:69
  271.6 64.7 %collective-permute-start.34 = (bf16[512,1024]{1,0:T(8,128)(2,1)S(1)}, bf16[512,1024]{1,0:T(8,128)(2,1)S(1)}, u32[]{:S(2)}, u32[]{:S(2)}) collective-permute-start(bf16[512,1024]{1,0:T(8,128)(2,1)S(1)} %bitcast.227), channel_id=1, source_target_pairs={{8,0},{10,2},{12,4},{14,6},{16,8},{18,10},{20,12},{22,14},{24,16},... | collective-permute-start | bytes 3145736 | tf_op jit(solution)/shard_map/ppermute | solution.py:69
  291.5 44.8 %collective-permute-start.33 = (bf16[512,1024]{1,0:T(8,128)(2,1)}, bf16[512,1024]{1,0:T(8,128)(2,1)S(1)}, u32[]{:S(2)}, u32[]{:S(2)}) collective-permute-start(bf16[512,1024]{1,0:T(8,128)(2,1)} %collective-permute-done.32), channel_id=1, source_target_pairs={{16,24},{18,26},{20,28},{22,30},{17,25},{19,27},{21,29},{23,31}} | collective-permute-start | bytes 3145736 | tf_op jit(solution)/shard_map/ppermute | solution.py:69
  293.9 64.8 %collective-permute-start.44 = (bf16[1024,512]{0,1:T(8,128)(2,1)S(1)}, bf16[1024,512]{0,1:T(8,128)(2,1)S(1)}, u32[]{:S(2)}, u32[]{:S(2)}) collective-permute-start(bf16[1024,512]{0,1:T(8,128)(2,1)S(1)} %bitcast.232), channel_id=1, source_target_pairs={{8,0},{10,2},{12,4},{14,6},{16,8},{18,10},{20,12},{22,14},{24,16},... | collective-permute-start | bytes 3145736 | tf_op jit(solution)/shard_map/ppermute | solution.py:69
  313.9 44.7 %collective-permute-start.43 = (bf16[1024,512]{0,1:T(8,128)(2,1)}, bf16[1024,512]{0,1:T(8,128)(2,1)S(1)}, u32[]{:S(2)}, u32[]{:S(2)}) collective-permute-start(bf16[1024,512]{0,1:T(8,128)(2,1)} %collective-permute-done.42), channel_id=1, source_target_pairs={{16,24},{18,26},{20,28},{22,30},{17,25},{19,27},{21,29},{23,31}} | collective-permute-start | bytes 3145736 | tf_op jit(solution)/shard_map/ppermute | solution.py:69
  384.1 19.5 %collective-permute-start.49 = (bf16[2,384,512]{2,1,0:T(8,128)(2,1)S(1)}, bf16[2,384,512]{2,1,0:T(8,128)(2,1)S(1)}, u32[]{:S(2)}, u32[]{:S(2)}) collective-permute-start(bf16[2,384,512]{2,1,0:T(8,128)(2,1)S(1)} %pad_maximum_fusion.1), channel_id=1, source_target_pairs={{0,4},{2,6},{4,0},{6,2},{8,12},{10,14},{12,8},{14,10},{16,20},{18,... | collective-permute-start | bytes 2359304 | tf_op jit(solution)/shard_map/ppermute | solution.py:61
  389.1 20.5 %collective-permute-start.46 = (bf16[2,384,512]{2,1,0:T(8,128)(2,1)S(1)}, bf16[2,384,512]{2,1,0:T(8,128)(2,1)S(1)}, u32[]{:S(2)}, u32[]{:S(2)}) collective-permute-start(bf16[2,384,512]{2,1,0:T(8,128)(2,1)S(1)} %pad_maximum_fusion), channel_id=1, source_target_pairs={{0,2},{2,0},{4,6},{6,4},{8,10},{10,8},{12,14},{14,12},{16,18},{18,... | collective-permute-start | bytes 2359304 | tf_op jit(solution)/shard_map/ppermute | solution.py:61
  (41 other events, 331.4 us)
where the time goes:
time: 425 us; the launch traced here: 423 us
  waiting for transfers between devices  224 us (53%)
  starting transfers between devices  103 us (24%)
  matrix products  34 us (8%)
  local copies, waits for them, and re-layouts  30.9 us (7%)
  other arithmetic  22.2 us (5%)
  blocking collectives  7.7 us (2%)
    ppermute x24, waiting for transfers between devices, shift(): return lax.ppermute(array, 'fs', pairs)  129 us
    ppermute x22, waiting for transfers between devices, swap(): return lax.ppermute(array, 'fs', pairs)  94.3 us
    ppermute x24, starting transfers between devices, shift(): return lax.ppermute(array, 'fs', pairs)  74.3 us
    ppermute x22, starting transfers between devices, swap(): return lax.ppermute(array, 'fs', pairs)  27.8 us
    dot_general x6, matrix products, tp_dot(): term = jnp.dot(piece, rows_at, preferred_element_type=jnp.float32)  18 us
    dot_general x4, matrix products, product(): return jnp.dot(hidden, weights, preferred_element_type=jnp.float32)  16 us
    dynamic_update_slice x16, other arithmetic, put(): lax.dynamic_update_slice_in_dim(buffer, jnp.expand_dims(block, axis), ind...  12.1 us
    dynamic_update_slice x20, local copies, waits for them, and re-layouts, put(): lax.dynamic_update_slice_in_dim(buffer, jnp.expand_dims(block, axis), ind...  11.4 us
  transfers between devices with their start and end apart: 51, of which 26 were waited for; matrix products, arithmetic and copies ran while one was open for 13% of the time, Pallas kernels for 0%

commit v1 on v0

--- a/solution.py
+++ b/solution.py
@@ -60,30 +60,23 @@
         pairs = [(f, (f // PLANE) * PLANE + ((f % PLANE) ^ mask)) for f in range(n_fs)]
         return lax.ppermute(array, "fs", pairs)
 
-    def shift(array, step, upward, first=0):
-        if upward:
-            moves = [(a, a + step) for a in range(first, lines - step)]
-        else:
-            moves = [(a, a - step) for a in range(step, lines - first)]
-        pairs = [(a * PLANE + q, b * PLANE + q) for a, b in moves for q in range(PLANE)]
+    def cross(array, mask):
+        pairs = [(f, ((f // PLANE) ^ mask) * PLANE + f % PLANE) for f in range(n_fs)]
         return lax.ppermute(array, "fs", pairs)
 
     def put(buffer, block, index, axis=0):
         return lax.dynamic_update_slice_in_dim(buffer, jnp.expand_dims(block, axis), index, axis)
 
-    def line_gather(block, direct):
-        ups, downs = [block], [block]
-        for step in range(1, lines):
-            if step <= direct:
-                ups.append(shift(block, step, True))
-                downs.append(shift(block, step, False))
-            else:
-                ups.append(shift(ups[-1], 1, True, step - 1))
-                downs.append(shift(downs[-1], 1, False, step - 1))
-        out = put(jnp.zeros((lines,) + block.shape, block.dtype), block, line)
-        for step in range(1, lines):
-            piece = jnp.where(line >= step, ups[step], downs[lines - step])
-            out = put(out, piece, (line - step) % lines)
+    def line_gather(block):
+        held = {0: block}
+        mask = lines // 2
+        while mask:
+            for at, piece in list(held.items()):
+                held[at ^ mask] = cross(piece, mask)
+            mask //= 2
+        out = jnp.zeros((lines,) + block.shape, block.dtype)
+        for at, piece in held.items():
+            out = put(out, piece, line ^ at)
         return out
 
     def plane_gather(block, axis):
@@ -119,19 +112,19 @@
         return out
 
     pair_block = jnp.concatenate([w_value, w_gate], 1)
-    pair_whole = plane_gather(line_gather(pair_block, lines), 1).reshape(width, 2 * channel_part)
+    pair_whole = plane_gather(line_gather(pair_block), 1).reshape(width, 2 * channel_part)
     rows = w_value.shape[0]
-    mix_whole = plane_gather(line_gather(w_mix_out, lines), 1).reshape(channels, width_part)
+    mix_whole = plane_gather(line_gather(w_mix_out), 1).reshape(channels, width_part)
 
     units = w_up.shape[1]
     quarter = units // PLANE
     up_pieces = jnp.swapaxes(w_up.reshape(rows, PLANE, quarter), 0, 1)
     up_chunk = plane_exchange(up_pieces).reshape(PLANE * rows, quarter)
-    up_whole = line_gather(up_chunk, 2).reshape(width, quarter)
+    up_whole = line_gather(up_chunk).reshape(width, quarter)
     cols = w_down.shape[1]
     down_pieces = w_down.reshape(PLANE, quarter, cols)
     down_chunk = jnp.swapaxes(plane_exchange(down_pieces), 0, 1).reshape(quarter, PLANE * cols)
-    down_whole = line_gather(down_chunk, 2)
+    down_whole = line_gather(down_chunk)
 
     both = tp_dot(tokens, pair_whole)
     values_proj, gate_proj = both[:, :channel_part], both[:, channel_part:]

time: 425 us -> 360 us (0.85)
  starting transfers between devices: 103 us -> 41.4 us
  other arithmetic: 22.2 us -> 9.93 us
  local copies, waits for them, and re-layouts: 30.9 us -> 40.9 us
    ppermute x24 -> x12, starting transfers between devices: 74.3 us -> 16.3 us  [cross(): return lax.ppermute(array, 'fs', pairs)]
    dynamic_update_slice x16 -> x4, other arithmetic: 12.1 us -> 2.32 us  [put(): lax.dynamic_update_slice_in_dim(buffer, jnp.expand_dims(block, axis), ind...]
    dynamic_update_slice x20 -> x32, local copies, waits for them, and re-layouts: 11.4 us -> 19.4 us  [put(): lax.dynamic_update_slice_in_dim(buffer, jnp.expand_dims(block, axis), ind...]
    ppermute x24 -> x12, waiting for transfers between devices: 129 us -> 136 us  [cross(): return lax.ppermute(array, 'fs', pairs)]
    ppermute x22, waiting for transfers between devices: 94.3 us -> 88.4 us  [swap(): return lax.ppermute(array, 'fs', pairs)]
  transfers between devices with their start and end apart: 51 -> 39, of which waited for: 26 -> 20; matrix products, arithmetic and copies ran while one was open for 13% -> 17% of each run, Pallas kernels for 0% -> 0%
where the time goes in v1:
time: 360 us; the launch traced here: 359 us
  waiting for transfers between devices  225 us (62%)
  starting transfers between devices  41.4 us (12%)
  local copies, waits for them, and re-layouts  40.9 us (11%)
  matrix products  33.5 us (9%)
  other arithmetic  9.93 us (3%)
  blocking collectives  7.7 us (2%)
    ppermute x12, waiting for transfers between devices, cross(): return lax.ppermute(array, 'fs', pairs)  136 us
    ppermute x22, waiting for transfers between devices, swap(): return lax.ppermute(array, 'fs', pairs)  88.4 us
    ppermute x22, starting transfers between devices, swap(): return lax.ppermute(array, 'fs', pairs)  24.3 us
    dynamic_update_slice x32, local copies, waits for them, and re-layouts, put(): lax.dynamic_update_slice_in_dim(buffer, jnp.expand_dims(block, axis), ind...  19.4 us
    dot_general x6, matrix products, tp_dot(): term = jnp.dot(piece, rows_at, preferred_element_type=jnp.float32)  17.6 us
    ppermute x12, starting transfers between devices, cross(): return lax.ppermute(array, 'fs', pairs)  16.3 us
    dot_general x4, matrix products, product(): return jnp.dot(hidden, weights, preferred_element_type=jnp.float32)  16 us
  transfers between devices with their start and end apart: 39, of which 20 were waited for; matrix products, arithmetic and copies ran while one was open for 17% of the time, Pallas kernels for 0%

profile of v1, /device:TPU:0, one launch (start us, length us, event | category | flops | bytes accessed | tf_op | source)
XLA Modules:
  0.0 359.3 jit_solution(15244474960986733270)
XLA Ops:
  3.2 4.1 %collective-permute-start = (bf16[128,1024]{1,0:T(8,128)(2,1)}, bf16[128,1024]{1,0:T(8,128)(2,1)}, u32[]{:S(2)}, u32[]{:S(2)}) collective-permute-start(bf16[128,1024]{1,0:T(8,128)(2,1)} %constant_dynamic-update-slice_fusion.4), channel_id=1, source_target_pairs={{0,16},{2,18},{4,20},{6,22},{8,24},{10,26},{12,28},{14,30},{16,0},... | collective-permute-start | bytes 786440 | tf_op jit(solution)/shard_map/ppermute | solution.py:65
  12.8 1.8 collective-permute-start.20
  21.4 3.9 %collective-permute-done.8 = bf16[64,1024]{1,0:T(8,128)(2,1)} collective-permute-done((bf16[64,1024]{1,0:T(8,128)(2,1)}, bf16[64,1024]{1,0:T(8,128)(2,1)}, u32[]{:S(2)}, u32[]{:S(2)}) %collective-permute-start.8) | collective-permute-done | bytes 131104 | tf_op jit(solution)/shard_map/ppermute | solution.py:65
  37.2 3.6 collective-permute-done.2
  43.8 3.8 %collective-permute-done.12 = bf16[4,64,1024]{2,1,0:T(8,128)(2,1)S(1)} collective-permute-done((bf16[4,64,1024]{2,1,0:T(8,128)(2,1)}, bf16[4,64,1024]{2,1,0:T(8,128)(2,1)S(1)}, u32[]{:S(2)}, u32[]{:S(2)}) %collective-permute-start.12) | collective-permute-done | bytes 524320 | tf_op jit(solution)/shard_map/ppermute | solution.py:61
  50.0 21.6 %collective-permute-done.13 = bf16[2,64,1024]{2,1,0:T(8,128)(2,1)S(1)} collective-permute-done((bf16[2,64,1024]{2,1,0:T(8,128)(2,1)S(1)}, bf16[2,64,1024]{2,1,0:T(8,128)(2,1)S(1)}, u32[]{:S(2)}, u32[]{:S(2)}) %collective-permute-start.13) | collective-permute-done | bytes 262176 | tf_op jit(solution)/shard_map/ppermute | solution.py:61
  75.8 12.4 %collective-permute-done.5 = bf16[2,128,1024]{2,1,0:T(8,128)(2,1)S(1)} collective-permute-done((bf16[2,128,1024]{2,1,0:T(8,128)(2,1)S(1)}, bf16[2,128,1024]{2,1,0:T(8,128)(2,1)S(1)}, u32[]{:S(2)}, u32[]{:S(2)}) %collective-permute-start.5) | collective-permute-done | bytes 524320 | tf_op jit(solution)/shard_map/ppermute | solution.py:61
  92.1 3.5 fusion.118
  95.6 2.5 all-reduce.3
  100.2 1.9 fusion.117
  102.2 2.8 all-reduce.2
  104.9 2.1 broadcast_in_dim.178
  114.8 15.5 %collective-permute-done.17 = bf16[384,1024]{1,0:T(8,128)(2,1)S(1)} collective-permute-done((bf16[384,1024]{1,0:T(8,128)(2,1)S(1)}, bf16[384,1024]{1,0:T(8,128)(2,1)S(1)}, u32[]{:S(2)}, u32[]{:S(2)}) %collective-permute-start.17) | collective-permute-done | bytes 786464 | tf_op jit(solution)/shard_map/ppermute | solution.py:61
  134.4 7.6 %collective-permute-done.18 = bf16[192,1024]{1,0:T(8,128)(2,1)S(1)} collective-permute-done((bf16[192,1024]{1,0:T(8,128)(2,1)S(1)}, bf16[192,1024]{1,0:T(8,128)(2,1)S(1)}, u32[]{:S(2)}, u32[]{:S(2)}) %collective-permute-start.18) | collective-permute-done | bytes 393248 | tf_op jit(solution)/shard_map/ppermute | solution.py:61
  142.0 2.1 collective-permute-start.29
  146.0 4.3 %collective-permute-start.23 = (bf16[512,1024]{1,0:T(8,128)(2,1)S(1)}, bf16[512,1024]{1,0:T(8,128)(2,1)}, u32[]{:S(2)}, u32[]{:S(2)}) collective-permute-start(bf16[512,1024]{1,0:T(8,128)(2,1)S(1)} %bitcast.219), channel_id=1, source_target_pairs={{0,16},{2,18},{4,20},{6,22},{8,24},{10,26},{12,28},{14,30},{16,0},... | collective-permute-start | bytes 3145736 | tf_op jit(solution)/shard_map/ppermute | solution.py:65
  160.9 58.6 %collective-permute-done.23 = bf16[512,1024]{1,0:T(8,128)(2,1)} collective-permute-done((bf16[512,1024]{1,0:T(8,128)(2,1)S(1)}, bf16[512,1024]{1,0:T(8,128)(2,1)}, u32[]{:S(2)}, u32[]{:S(2)}) %collective-permute-start.23) | collective-permute-done | bytes 1048608 | tf_op jit(solution)/shard_map/ppermute | solution.py:65
  220.0 21.8 %collective-permute-done.30 = bf16[1024,512]{0,1:T(8,128)(2,1)} collective-permute-done((bf16[1024,512]{0,1:T(8,128)(2,1)S(1)}, bf16[1024,512]{0,1:T(8,128)(2,1)}, u32[]{:S(2)}, u32[]{:S(2)}) %collective-permute-start.30) | collective-permute-done | bytes 1048608 | tf_op jit(solution)/shard_map/ppermute | solution.py:65
  246.1 4.2 %collective-permute-done.31 = bf16[1024,512]{0,1:T(8,128)(2,1)S(1)} collective-permute-done((bf16[1024,512]{0,1:T(8,128)(2,1)S(1)}, bf16[1024,512]{0,1:T(8,128)(2,1)S(1)}, u32[]{:S(2)}, u32[]{:S(2)}) %collective-permute-start.31) | collective-permute-done | bytes 1048608 | tf_op jit(solution)/shard_map/ppermute | solution.py:65
  250.4 22.4 %collective-permute-done.25 = bf16[512,1024]{1,0:T(8,128)(2,1)S(1)} collective-permute-done((bf16[512,1024]{1,0:T(8,128)(2,1)}, bf16[512,1024]{1,0:T(8,128)(2,1)S(1)}, u32[]{:S(2)}, u32[]{:S(2)}) %collective-permute-start.25) | collective-permute-done | bytes 1048608 | tf_op jit(solution)/shard_map/ppermute | solution.py:65
  272.9 20.2 %collective-permute-done.32 = bf16[1024,512]{0,1:T(8,128)(2,1)S(1)} collective-permute-done((bf16[1024,512]{0,1:T(8,128)(2,1)}, bf16[1024,512]{0,1:T(8,128)(2,1)S(1)}, u32[]{:S(2)}, u32[]{:S(2)}) %collective-permute-start.32) | collective-permute-done | bytes 1048608 | tf_op jit(solution)/shard_map/ppermute | solution.py:65
  293.3 6.9 %fusion = f32[1536,1024]{1,0:T(8,128)S(1)} fusion(bf16[1536,1024]{1,0:T(8,128)(2,1)} %collective-permute-done.26, bf16[2,1024,1024]{2,1,0:T(8,128)(2,1)S(1)} %bitcast.225, s32[]{:T(128)S(6)} %select_n.151), kind=kOutput, calls=%fused_computation.35 | convolution fusion | flops 3221225472 | bytes 11534340 | tf_op jit(solution)/shard_map/dot_general | solution.py:101
  300.2 6.1 %multiply_convert_fusion = bf16[1536,1024]{1,0:T(8,128)(2,1)S(1)} fusion(f32[1536,1024]{1,0:T(8,128)S(1)} %fusion, bf16[1536,1024]{1,0:T(8,128)(2,1)} %bitcast.72, bf16[2,1024,1024]{2,1,0:T(8,128)(2,1)S(1)} %bitcast.226, s32[]{:T(128)S(6)} %select_n.149), kind=kOutput, calls=%fused_computation | convolution fusion | flops 3227516928 | bytes 14680068 | tf_op jit(solution)/shard_map/dot_general | solution.py:101
  306.3 3.0 convolution_convert_fusion.1
  309.4 5.2 %convolution_convert_fusion = bf16[1536,512]{1,0:T(8,128)(2,1)} fusion(bf16[1536,1024]{1,0:T(8,128)(2,1)} %copy-done.14, bf16[4,1024,512]{1,2,0:T(8,128)(2,1)} %copy-done.1, s32[]{:T(128)S(6)} %select_n.157), kind=kOutput, calls=%fused_computation.3 | convolution fusion | flops 1611399168 | bytes 5767172 | tf_op jit(solution)/shard_map/dot_general | solution.py:154
  315.1 4.6 %convolution_add_fusion.1 = f32[1536,512]{1,0:T(8,128)S(1)} fusion(bf16[1536,1024]{1,0:T(8,128)(2,1)} %copy-done.14, bf16[1536,512]{1,0:T(8,128)(2,1)} %collective-permute-done.33, bf16[4,1024,512]{1,2,0:T(8,128)(2,1)} %copy-done.1, s32[]{:T(128)S(6)} %select_n.153), kind=kOutput, calls=%fused_computation.2 | convolution fusion | flops 1612185600 | bytes 8912900 | tf_op jit(solution)/shard_map/dot_general | solution.py:154
  321.6 3.1 convolution_add_fusion
  325.8 13.7 %collective-permute-done.34 = bf16[2,384,512]{2,1,0:T(8,128)(2,1)S(1)} collective-permute-done((bf16[2,384,512]{2,1,0:T(8,128)(2,1)S(1)}, bf16[2,384,512]{2,1,0:T(8,128)(2,1)S(1)}, u32[]{:S(2)}, u32[]{:S(2)}) %collective-permute-start.34) | collective-permute-done | bytes 786464 | tf_op jit(solution)/shard_map/ppermute | solution.py:61
  340.6 4.8 %collective-permute-done.37 = bf16[2,384,512]{2,1,0:T(8,128)(2,1)S(1)} collective-permute-done((bf16[2,384,512]{2,1,0:T(8,128)(2,1)S(1)}, bf16[2,384,512]{2,1,0:T(8,128)(2,1)S(1)}, u32[]{:S(2)}, u32[]{:S(2)}) %collective-permute-start.37) | collective-permute-done | bytes 786464 | tf_op jit(solution)/shard_map/ppermute | solution.py:61
  346.5 6.3 %collective-permute-done.35 = bf16[384,512]{1,0:T(8,128)(2,1)S(1)} collective-permute-done((bf16[384,512]{1,0:T(8,128)(2,1)S(1)}, bf16[384,512]{1,0:T(8,128)(2,1)S(1)}, u32[]{:S(2)}, u32[]{:S(2)}) %collective-permute-start.35) | collective-permute-done | bytes 393248 | tf_op jit(solution)/shard_map/ppermute | solution.py:61
  353.1 1.9 collective-permute-done.38
  355.6 2.5 all-reduce.1
  (182 shorter events, 79.6 us)
Async XLA Ops:
  3.2 31.0 %collective-permute-start = (bf16[128,1024]{1,0:T(8,128)(2,1)}, bf16[128,1024]{1,0:T(8,128)(2,1)}, u32[]{:S(2)}, u32[]{:S(2)}) collective-permute-start(bf16[128,1024]{1,0:T(8,128)(2,1)} %constant_dynamic-update-slice_fusion.4), channel_id=1, source_target_pairs={{0,16},{2,18},{4,20},{6,22},{8,24},{10,26},{12,28},{14,30},{16,0},... | collective-permute-start | bytes 786440 | tf_op jit(solution)/shard_map/ppermute | solution.py:65
  7.2 28.9 %collective-permute-start.1 = (bf16[128,1024]{1,0:T(8,128)(2,1)}, bf16[128,1024]{1,0:T(8,128)(2,1)}, u32[]{:S(2)}, u32[]{:S(2)}) collective-permute-start(bf16[128,1024]{1,0:T(8,128)(2,1)} %constant_dynamic-update-slice_fusion.4), channel_id=1, source_target_pairs={{0,8},{2,10},{4,12},{6,14},{8,0},{10,2},{12,4},{14,6},{16,24},{18,... | collective-permute-start | bytes 786440 | tf_op jit(solution)/shard_map/ppermute | solution.py:65
  8.8 16.4 %collective-permute-start.8 = (bf16[64,1024]{1,0:T(8,128)(2,1)}, bf16[64,1024]{1,0:T(8,128)(2,1)}, u32[]{:S(2)}, u32[]{:S(2)}) collective-permute-start(bf16[64,1024]{1,0:T(8,128)(2,1)} %param.15), channel_id=1, source_target_pairs={{0,16},{2,18},{4,20},{6,22},{8,24},{10,26},{12,28},{14,30},{16,0},... | collective-permute-start | bytes 393224 | tf_op jit(solution)/shard_map/ppermute | solution.py:65
  9.1 18.3 %collective-permute-start.9 = (bf16[64,1024]{1,0:T(8,128)(2,1)}, bf16[64,1024]{1,0:T(8,128)(2,1)}, u32[]{:S(2)}, u32[]{:S(2)}) collective-permute-start(bf16[64,1024]{1,0:T(8,128)(2,1)} %param.15), channel_id=1, source_target_pairs={{0,8},{2,10},{4,12},{6,14},{8,0},{10,2},{12,4},{14,6},{16,24},{18,... | collective-permute-start | bytes 393224 | tf_op jit(solution)/shard_map/ppermute | solution.py:65
  12.8 98.6 %collective-permute-start.20 = (bf16[128,1024]{1,0:T(8,128)(2,1)}, bf16[128,1024]{1,0:T(8,128)(2,1)}, u32[]{:S(2)}, u32[]{:S(2)}) collective-permute-start(bf16[128,1024]{1,0:T(8,128)(2,1)} %bitcast.75), channel_id=1, source_target_pairs={{0,2},{2,0},{4,6},{6,4},{8,10},{10,8},{12,14},{14,12},{16,18},{18,... | collective-permute-start | bytes 786440 | tf_op jit(solution)/shard_map/ppermute | solution.py:61
  31.1 17.1 %collective-permute-start.11 = (bf16[4,64,1024]{2,1,0:T(8,128)(2,1)}, bf16[4,64,1024]{2,1,0:T(8,128)(2,1)S(1)}, u32[]{:S(2)}, u32[]{:S(2)}) collective-permute-start(bf16[4,64,1024]{2,1,0:T(8,128)(2,1)} %bitcast_dynamic-update-slice_fusion.25), channel_id=1, source_target_pairs={{0,2},{2,0},{4,6},{6,4},{8,10},{10,8},{12,14},{14,12},{16,18},{18,... | collective-permute-start | bytes 1572872 | tf_op jit(solution)/shard_map/ppermute | solution.py:61
  32.6 15.0 %collective-permute-start.12 = (bf16[4,64,1024]{2,1,0:T(8,128)(2,1)}, bf16[4,64,1024]{2,1,0:T(8,128)(2,1)S(1)}, u32[]{:S(2)}, u32[]{:S(2)}) collective-permute-start(bf16[4,64,1024]{2,1,0:T(8,128)(2,1)} %bitcast_dynamic-update-slice_fusion.25), channel_id=1, source_target_pairs={{0,4},{2,6},{4,0},{6,2},{8,12},{10,14},{12,8},{14,10},{16,20},{18,... | collective-permute-start | bytes 1572872 | tf_op jit(solution)/shard_map/ppermute | solution.py:61
  40.7 34.0 %collective-permute-start.3 = (bf16[4,128,1024]{2,1,0:T(8,128)(2,1)S(1)}, bf16[4,128,1024]{2,1,0:T(8,128)(2,1)S(1)}, u32[]{:S(2)}, u32[]{:S(2)}) collective-permute-start(bf16[4,128,1024]{2,1,0:T(8,128)(2,1)S(1)} %bitcast_dynamic-update-slice_fusion.21), channel_id=1, source_target_pairs={{0,2},{2,0},{4,6},{6,4},{8,10},{10,8},{12,14},{14,12},{16,18},{18,... | collective-permute-start | bytes 3145736 | tf_op jit(solution)/shard_map/ppermute | solution.py:61
  41.3 32.4 %collective-permute-start.4 = (bf16[4,128,1024]{2,1,0:T(8,128)(2,1)S(1)}, bf16[4,128,1024]{2,1,0:T(8,128)(2,1)S(1)}, u32[]{:S(2)}, u32[]{:S(2)}) collective-permute-start(bf16[4,128,1024]{2,1,0:T(8,128)(2,1)S(1)} %bitcast_dynamic-update-slice_fusion.21), channel_id=1, source_target_pairs={{0,4},{2,6},{4,0},{6,2},{8,12},{10,14},{12,8},{14,10},{16,20},{18,... | collective-permute-start | bytes 3145736 | tf_op jit(solution)/shard_map/ppermute | solution.py:61
  47.6 23.9 %collective-permute-start.13 = (bf16[2,64,1024]{2,1,0:T(8,128)(2,1)S(1)}, bf16[2,64,1024]{2,1,0:T(8,128)(2,1)S(1)}, u32[]{:S(2)}, u32[]{:S(2)}) collective-permute-start(bf16[2,64,1024]{2,1,0:T(8,128)(2,1)S(1)} %slice.297), channel_id=1, source_target_pairs={{0,2},{2,0},{4,6},{6,4},{8,10},{10,8},{12,14},{14,12},{16,18},{18,... | collective-permute-start | bytes 786440 | tf_op jit(solution)/shard_map/ppermute | solution.py:61
  48.2 25.5 %collective-permute-start.14 = (bf16[2,64,1024]{2,1,0:T(8,128)(2,1)S(1)}, bf16[2,64,1024]{2,1,0:T(8,128)(2,1)S(1)}, u32[]{:S(2)}, u32[]{:S(2)}) collective-permute-start(bf16[2,64,1024]{2,1,0:T(8,128)(2,1)S(1)} %slice.298), channel_id=1, source_target_pairs={{0,4},{2,6},{4,0},{6,2},{8,12},{10,14},{12,8},{14,10},{16,20},{18,... | collective-permute-start | bytes 786440 | tf_op jit(solution)/shard_map/ppermute | solution.py:61
  71.6 41.6 %collective-permute-start.21 = (bf16[128,1024]{1,0:T(8,128)(2,1)}, bf16[128,1024]{1,0:T(8,128)(2,1)}, u32[]{:S(2)}, u32[]{:S(2)}) collective-permute-start(bf16[128,1024]{1,0:T(8,128)(2,1)} %bitcast.77), channel_id=1, source_target_pairs={{0,4},{2,6},{4,0},{6,2},{8,12},{10,14},{12,8},{14,10},{16,20},{18,... | collective-permute-start | bytes 786440 | tf_op jit(solution)/shard_map/ppermute | solution.py:61
  73.7 16.1 %collective-permute-start.7 = (bf16[384,1024]{1,0:T(8,128)(2,1)S(1)}, bf16[384,1024]{1,0:T(8,128)(2,1)S(1)}, u32[]{:S(2)}, u32[]{:S(2)}) collective-permute-start(bf16[384,1024]{1,0:T(8,128)(2,1)S(1)} %copy-done.2), channel_id=1, source_target_pairs={{0,1},{1,0},{2,3},{3,2},{4,5},{5,4},{6,7},{7,6},{8,9},{9,8},{10,11... | collective-permute-start | bytes 2359304 | tf_op jit(solution)/shard_map/ppermute | solution.py:93
  73.8 14.4 %collective-permute-start.5 = (bf16[2,128,1024]{2,1,0:T(8,128)(2,1)S(1)}, bf16[2,128,1024]{2,1,0:T(8,128)(2,1)S(1)}, u32[]{:S(2)}, u32[]{:S(2)}) collective-permute-start(bf16[2,128,1024]{2,1,0:T(8,128)(2,1)S(1)} %slice.293), channel_id=1, source_target_pairs={{0,2},{2,0},{4,6},{6,4},{8,10},{10,8},{12,14},{14,12},{16,18},{18,... | collective-permute-start | bytes 1572872 | tf_op jit(solution)/shard_map/ppermute | solution.py:61
  74.8 14.8 %collective-permute-start.6 = (bf16[2,128,1024]{2,1,0:T(8,128)(2,1)S(1)}, bf16[2,128,1024]{2,1,0:T(8,128)(2,1)S(1)}, u32[]{:S(2)}, u32[]{:S(2)}) collective-permute-start(bf16[2,128,1024]{2,1,0:T(8,128)(2,1)S(1)} %slice.294), channel_id=1, source_target_pairs={{0,4},{2,6},{4,0},{6,2},{8,12},{10,14},{12,8},{14,10},{16,20},{18,... | collective-permute-start | bytes 1572872 | tf_op jit(solution)/shard_map/ppermute | solution.py:61
  88.2 56.9 %collective-permute-start.22 = (bf16[128,1024]{1,0:T(8,128)(2,1)}, bf16[128,1024]{1,0:T(8,128)(2,1)}, u32[]{:S(2)}, u32[]{:S(2)}) collective-permute-start(bf16[128,1024]{1,0:T(8,128)(2,1)} %bitcast.79), channel_id=1, source_target_pairs={{0,6},{2,4},{4,2},{6,0},{8,14},{10,12},{12,10},{14,8},{16,22},{18,... | collective-permute-start | bytes 786440 | tf_op jit(solution)/shard_map/ppermute | solution.py:61
  108.3 22.5 %collective-permute-start.16 = (bf16[384,1024]{1,0:T(8,128)(2,1)S(1)}, bf16[384,1024]{1,0:T(8,128)(2,1)S(1)}, u32[]{:S(2)}, u32[]{:S(2)}) collective-permute-start(bf16[384,1024]{1,0:T(8,128)(2,1)S(1)} %get-tuple-element.18), channel_id=1, source_target_pairs={{0,2},{2,0},{4,6},{6,4},{8,10},{10,8},{12,14},{14,12},{16,18},{18,... | collective-permute-start | bytes 2359304 | tf_op jit(solution)/shard_map/ppermute | solution.py:61
  109.9 20.4 %collective-permute-start.17 = (bf16[384,1024]{1,0:T(8,128)(2,1)S(1)}, bf16[384,1024]{1,0:T(8,128)(2,1)S(1)}, u32[]{:S(2)}, u32[]{:S(2)}) collective-permute-start(bf16[384,1024]{1,0:T(8,128)(2,1)S(1)} %get-tuple-element.18), channel_id=1, source_target_pairs={{0,4},{2,6},{4,0},{6,2},{8,12},{10,14},{12,8},{14,10},{16,20},{18,... | collective-permute-start | bytes 2359304 | tf_op jit(solution)/shard_map/ppermute | solution.py:61
  111.4 39.0 %collective-permute-start.27 = (bf16[1024,128]{1,0:T(8,128)(2,1)S(1)}, bf16[1024,128]{1,0:T(8,128)(2,1)S(1)}, u32[]{:S(2)}, u32[]{:S(2)}) collective-permute-start(bf16[1024,128]{1,0:T(8,128)(2,1)S(1)} %copy-done.9), channel_id=1, source_target_pairs={{0,2},{2,0},{4,6},{6,4},{8,10},{10,8},{12,14},{14,12},{16,18},{18,... | collective-permute-start | bytes 786440 | tf_op jit(solution)/shard_map/ppermute | solution.py:61
  113.2 38.9 %collective-permute-start.28 = (bf16[1024,128]{1,0:T(8,128)(2,1)S(1)}, bf16[1024,128]{1,0:T(8,128)(2,1)}, u32[]{:S(2)}, u32[]{:S(2)}) collective-permute-start(bf16[1024,128]{1,0:T(8,128)(2,1)S(1)} %copy-done.8), channel_id=1, source_target_pairs={{0,4},{2,6},{4,0},{6,2},{8,12},{10,14},{12,8},{14,10},{16,20},{18,... | collective-permute-start | bytes 786440 | tf_op jit(solution)/shard_map/ppermute | solution.py:61
  130.4 11.6 %collective-permute-start.18 = (bf16[192,1024]{1,0:T(8,128)(2,1)S(1)}, bf16[192,1024]{1,0:T(8,128)(2,1)S(1)}, u32[]{:S(2)}, u32[]{:S(2)}) collective-permute-start(bf16[192,1024]{1,0:T(8,128)(2,1)S(1)} %slice.299), channel_id=1, source_target_pairs={{0,2},{2,0},{4,6},{6,4},{8,10},{10,8},{12,14},{14,12},{16,18},{18,... | collective-permute-start | bytes 1179656 | tf_op jit(solution)/shard_map/ppermute | solution.py:61
  130.9 13.2 %collective-permute-start.19 = (bf16[192,1024]{1,0:T(8,128)(2,1)S(1)}, bf16[192,1024]{1,0:T(8,128)(2,1)S(1)}, u32[]{:S(2)}, u32[]{:S(2)}) collective-permute-start(bf16[192,1024]{1,0:T(8,128)(2,1)S(1)} %slice.300), channel_id=1, source_target_pairs={{0,4},{2,6},{4,0},{6,2},{8,12},{10,14},{12,8},{14,10},{16,20},{18,... | collective-permute-start | bytes 1179656 | tf_op jit(solution)/shard_map/ppermute | solution.py:61
  145.1 148.2 %collective-permute-start.26 = (bf16[1536,1024]{1,0:T(8,128)(2,1)}, bf16[1536,1024]{1,0:T(8,128)(2,1)}, u32[]{:S(2)}, u32[]{:S(2)}) collective-permute-start(bf16[1536,1024]{1,0:T(8,128)(2,1)} %bitcast.72), channel_id=1, source_target_pairs={{0,1},{1,0},{2,3},{3,2},{4,5},{5,4},{6,7},{7,6},{8,9},{9,8},{10,11... | collective-permute-start | bytes 9437192 | tf_op jit(solution)/shard_map/ppermute | solution.py:93
  146.0 73.4 %collective-permute-start.23 = (bf16[512,1024]{1,0:T(8,128)(2,1)S(1)}, bf16[512,1024]{1,0:T(8,128)(2,1)}, u32[]{:S(2)}, u32[]{:S(2)}) collective-permute-start(bf16[512,1024]{1,0:T(8,128)(2,1)S(1)} %bitcast.219), channel_id=1, source_target_pairs={{0,16},{2,18},{4,20},{6,22},{8,24},{10,26},{12,28},{14,30},{16,0},... | collective-permute-start | bytes 3145736 | tf_op jit(solution)/shard_map/ppermute | solution.py:65
  156.1 85.7 %collective-permute-start.30 = (bf16[1024,512]{0,1:T(8,128)(2,1)S(1)}, bf16[1024,512]{0,1:T(8,128)(2,1)}, u32[]{:S(2)}, u32[]{:S(2)}) collective-permute-start(bf16[1024,512]{0,1:T(8,128)(2,1)S(1)} %bitcast.222), channel_id=1, source_target_pairs={{0,16},{2,18},{4,20},{6,22},{8,24},{10,26},{12,28},{14,30},{16,0},... | collective-permute-start | bytes 3145736 | tf_op jit(solution)/shard_map/ppermute | solution.py:65
  157.6 87.2 %collective-permute-start.24 = (bf16[512,1024]{1,0:T(8,128)(2,1)S(1)}, bf16[512,1024]{1,0:T(8,128)(2,1)}, u32[]{:S(2)}, u32[]{:S(2)}) collective-permute-start(bf16[512,1024]{1,0:T(8,128)(2,1)S(1)} %bitcast.220), channel_id=1, source_target_pairs={{0,8},{2,10},{4,12},{6,14},{8,0},{10,2},{12,4},{14,6},{16,24},{18,... | collective-permute-start | bytes 3145736 | tf_op jit(solution)/shard_map/ppermute | solution.py:65
  158.9 91.4 %collective-permute-start.31 = (bf16[1024,512]{0,1:T(8,128)(2,1)S(1)}, bf16[1024,512]{0,1:T(8,128)(2,1)S(1)}, u32[]{:S(2)}, u32[]{:S(2)}) collective-permute-start(bf16[1024,512]{0,1:T(8,128)(2,1)S(1)} %bitcast.223), channel_id=1, source_target_pairs={{0,8},{2,10},{4,12},{6,14},{8,0},{10,2},{12,4},{14,6},{16,24},{18,... | collective-permute-start | bytes 3145736 | tf_op jit(solution)/shard_map/ppermute | solution.py:65
  219.5 53.3 %collective-permute-start.25 = (bf16[512,1024]{1,0:T(8,128)(2,1)}, bf16[512,1024]{1,0:T(8,128)(2,1)S(1)}, u32[]{:S(2)}, u32[]{:S(2)}) collective-permute-start(bf16[512,1024]{1,0:T(8,128)(2,1)} %collective-permute-done.23), channel_id=1, source_target_pairs={{0,8},{2,10},{4,12},{6,14},{8,0},{10,2},{12,4},{14,6},{16,24},{18,... | collective-permute-start | bytes 3145736 | tf_op jit(solution)/shard_map/ppermute | solution.py:65
  241.8 51.4 %collective-permute-start.32 = (bf16[1024,512]{0,1:T(8,128)(2,1)}, bf16[1024,512]{0,1:T(8,128)(2,1)S(1)}, u32[]{:S(2)}, u32[]{:S(2)}) collective-permute-start(bf16[1024,512]{0,1:T(8,128)(2,1)} %collective-permute-done.30), channel_id=1, source_target_pairs={{0,8},{2,10},{4,12},{6,14},{8,0},{10,2},{12,4},{14,6},{16,24},{18,... | collective-permute-start | bytes 3145736 | tf_op jit(solution)/shard_map/ppermute | solution.py:65
  319.9 19.5 %collective-permute-start.34 = (bf16[2,384,512]{2,1,0:T(8,128)(2,1)S(1)}, bf16[2,384,512]{2,1,0:T(8,128)(2,1)S(1)}, u32[]{:S(2)}, u32[]{:S(2)}) collective-permute-start(bf16[2,384,512]{2,1,0:T(8,128)(2,1)S(1)} %pad_maximum_fusion), channel_id=1, source_target_pairs={{0,2},{2,0},{4,6},{6,4},{8,10},{10,8},{12,14},{14,12},{16,18},{18,... | collective-permute-start | bytes 2359304 | tf_op jit(solution)/shard_map/ppermute | solution.py:61
  324.9 20.5 %collective-permute-start.37 = (bf16[2,384,512]{2,1,0:T(8,128)(2,1)S(1)}, bf16[2,384,512]{2,1,0:T(8,128)(2,1)S(1)}, u32[]{:S(2)}, u32[]{:S(2)}) collective-permute-start(bf16[2,384,512]{2,1,0:T(8,128)(2,1)S(1)} %pad_maximum_fusion.1), channel_id=1, source_target_pairs={{0,4},{2,6},{4,0},{6,2},{8,12},{10,14},{12,8},{14,10},{16,20},{18,... | collective-permute-start | bytes 2359304 | tf_op jit(solution)/shard_map/ppermute | solution.py:61
  339.8 13.1 %collective-permute-start.35 = (bf16[384,512]{1,0:T(8,128)(2,1)S(1)}, bf16[384,512]{1,0:T(8,128)(2,1)S(1)}, u32[]{:S(2)}, u32[]{:S(2)}) collective-permute-start(bf16[384,512]{1,0:T(8,128)(2,1)S(1)} %fusion.102), channel_id=1, source_target_pairs={{0,4},{2,6},{4,0},{6,2},{8,12},{10,14},{12,8},{14,10},{16,20},{18,... | collective-permute-start | bytes 1179656 | tf_op jit(solution)/shard_map/ppermute | solution.py:61
  (25 other events, 172.5 us)
